TPU v7x, 32 devices: a whole 2x2x4 slice. The times are simulated.
32 devices in a mesh: sp: 4 (over x, core), dp: 8 (over z, y).
Axes of the slice: x: 2, y: 2, z: 4, core: 2. Of those that a mesh axis runs over, the one named last changes fastest.
Arguments:
- query: bfloat16 [8, 512, 1024], P('dp', None, 'sp'), may hold values from -120 to 120
- keys: bfloat16 [8, 512, 1024], P('dp', None, 'sp'), may hold values from -6 to 6
- values: bfloat16 [8, 512, 1024], P('dp', None, 'sp'), may hold values from -6 to 6
- output: bfloat16 [8, 512, 1024], P('dp'), may hold values from -1 to 1
- cum: float32 [8, 16, 512], P('dp', 'sp'), as said below
- d_out: bfloat16 [8, 512, 2048], P('dp', 'sp'), may hold values from -6 to 6
- w_out: bfloat16 [1024, 2048], P('dp'), may hold values from -0.125 to 0.125
Outputs:
- d_query: bfloat16 [8, 512, 1024], P('dp', 'sp')
- d_key: bfloat16 [8, 512, 1024], P('dp', 'sp')
- d_value: bfloat16 [8, 512, 1024], P('dp', 'sp')
- d_cum: float32 [8, 16, 512], P('dp', 'sp')
- d_w_out: float32 [1024, 2048], P('dp', 'sp')
Inputs may be any that keep to these rules, and one draw needn't show every extreme that they name: cum never rises along positions.
All inputs are finite; a program needn't handle non-finite values.
Results may differ from a plain program's by a relative error of at most 0.008.
Values may be sent and summed in bfloat16 or wider, within the bound.
A program may use at most 64 MiB of HBM per device.

v0:
```python
import jax
import jax.numpy as jnp
from jax import lax
from jax.sharding import PartitionSpec as P


def head_grads(query, keys, values, output, cotangent, cum):
    head_count, length, head_width = query.shape
    span_rows = min(512, length)
    score_scale = head_width ** (-0.5)
    row_dots = jnp.sum(cotangent.astype(jnp.float32) * output.astype(jnp.float32), axis=2)
    positions = jnp.arange(length)

    def product(left, right, form):
        return jnp.einsum(form, left, right, preferred_element_type=jnp.float32)

    def advance(totals, block_index):
        key_grad, value_grad, cum_grad = totals
        offset = block_index * span_rows
        query_blk = lax.dynamic_slice_in_dim(query, offset, span_rows, 1)
        cot_blk = lax.dynamic_slice_in_dim(cotangent, offset, span_rows, 1)
        cum_blk = lax.dynamic_slice_in_dim(cum, offset, span_rows, 1)
        dots_blk = lax.dynamic_slice_in_dim(row_dots, offset, span_rows, 1)
        scores = product(query_blk, keys, "hqe,hke->hqk") * score_scale
        scores = scores + cum_blk[:, :, None] - cum[:, None, :]
        query_pos = offset + jnp.arange(span_rows)
        causal = positions[None, :] <= query_pos[:, None]
        scores = jnp.where(causal[None], scores, -1e30)
        row_max = jnp.max(scores, axis=2, keepdims=True)
        weights = jnp.exp(scores - row_max)
        weights = weights / jnp.sum(weights, axis=2, keepdims=True)
        weights_b = weights.astype(jnp.bfloat16)
        d_prob = product(cot_blk, values, "hqe,hke->hqk")
        d_score = weights * (d_prob - dots_blk[:, :, None])
        score_b = d_score.astype(jnp.bfloat16)
        query_grad = (product(score_b, keys, "hqk,hke->hqe") * score_scale).astype(jnp.bfloat16)
        key_grad = key_grad + product(score_b, query_blk, "hqk,hqe->hke") * score_scale
        value_grad = value_grad + product(weights_b, cot_blk, "hqk,hqe->hke")
        cum_grad = cum_grad - jnp.sum(d_score, axis=1)
        own_part = lax.dynamic_slice_in_dim(cum_grad, offset, span_rows, 1) + jnp.sum(
            d_score, axis=2
        )
        cum_grad = lax.dynamic_update_slice_in_dim(cum_grad, own_part, offset, 1)
        return ((key_grad, value_grad, cum_grad), query_grad)

    start_state = (
        jnp.zeros(query.shape, jnp.float32),
        jnp.zeros(query.shape, jnp.float32),
        jnp.zeros(cum.shape, jnp.float32),
    )
    totals, query_blocks = lax.scan(advance, start_state, jnp.arange(length // span_rows))
    query_grad = jnp.transpose(query_blocks, (1, 0, 2, 3)).reshape(query.shape)
    return (query_grad, totals[0].astype(jnp.bfloat16), totals[1].astype(jnp.bfloat16), totals[2])


def shards(query, keys, values, output, cum, d_out, w_out):
    local_rows = d_out[0]
    whole_output = output[0]
    d_attn = lax.dot_general(
        local_rows,
        lax.all_gather(w_out, "dp", axis=0, tiled=True),
        (((1,), (1,)), ((), ())),
        preferred_element_type=jnp.float32,
    ).astype(jnp.bfloat16)
    head_cot, column_part = (
        lax.all_to_all(d_attn[None], "sp", split_axis=2, concat_axis=1, tiled=True),
        lax.all_to_all(d_out, "sp", split_axis=2, concat_axis=1, tiled=True),
    )
    grad_weight = lax.psum_scatter(
        lax.dot_general(
            whole_output,
            column_part[0],
            (((0,), (0,)), ((), ())),
            preferred_element_type=jnp.float32,
        ),
        "dp",
        scatter_dimension=0,
        tiled=True,
    )
    head_cols = query.shape[2]
    head_count = cum.shape[1]
    head_width = head_cols // head_count
    seq_length = query.shape[1]
    own_output = lax.dynamic_slice_in_dim(
        whole_output, lax.axis_index("sp") * head_cols, head_cols, 1
    )

    def heads_first(matrix):
        return jnp.transpose(matrix.reshape(seq_length, head_count, head_width), (1, 0, 2))

    def tokens_first(matrix):
        return jnp.transpose(matrix, (1, 0, 2)).reshape(1, seq_length, head_cols)

    grads = head_grads(
        heads_first(query[0]),
        heads_first(keys[0]),
        heads_first(values[0]),
        heads_first(own_output),
        heads_first(head_cot[0]),
        cum[0],
    )
    query_grad, key_grad, value_grad = (
        lax.all_to_all(tokens_first(grads[0]), "sp", split_axis=1, concat_axis=2, tiled=True),
        lax.all_to_all(tokens_first(grads[1]), "sp", split_axis=1, concat_axis=2, tiled=True),
        lax.all_to_all(tokens_first(grads[2]), "sp", split_axis=1, concat_axis=2, tiled=True),
    )
    return (query_grad, key_grad, value_grad, grads[3][None], grad_weight)


def solution(mesh):
    placed = (
        P("dp", None, "sp"),
        P("dp", None, "sp"),
        P("dp", None, "sp"),
        P("dp", None, None),
        P("dp", "sp", None),
        P("dp", "sp", None),
        P("dp", None),
    )
    return jax.shard_map(
        shards,
        mesh=mesh,
        in_specs=placed,
        out_specs=(
            P("dp", "sp", None),
            P("dp", "sp", None),
            P("dp", "sp", None),
            P("dp", "sp", None),
            P("dp", "sp"),
        ),
        check_vma=False,
    )
```

profile of v0, /device:TPU:0, one launch (start us, length us, event | category | flops | bytes accessed | tf_op | source)
XLA Modules:
  0.0 163.5 jit_solution(12182984740562545491)
XLA Ops:
  7.2 0.7 all-gather.2.cloned.1.call-update
  7.9 2.4 %copy.99 = bf16[1,128,2048]{1,0,2:T(2,128)(2,1)S(1)} copy(bf16[1,128,2048]{2,1,0:T(8,128)(2,1)} %param.12) | data formatting | bytes 1048576 | tf_op args[5]
  10.8 11.5 %reduce.4 = bf16[2048,128]{1,0:T(8,128)(2,1)S(1)} reduce(bf16[2048,1,128]{2,1,0:T(2,128)(2,1)S(1)} %bitcast.83, bf16[]{:T(256)} %broadcast.48), dimensions={1}, to_apply=%bitcast.67.reduce_sub_computation | reduce | bytes 1048578
  22.5 12.9 %all_to_all.84 = bf16[4,2,32768]{2,1,0:T(2,128)(2,1)S(1)} all-to-all(bf16[4,2,32768]{2,1,0:T(2,128)(2,1)S(1)} %reshape.79), channel_id=1, replica_groups=mesh['sp'=4,'dp'=8] {'sp'}, dimensions={0} | all-to-all | bytes 1048576 | tf_op jit(solution)/shard_map/all_to_all | solution.py:67
  36.2 2.1 %fusion.15 = f32[1024,512]{1,0:T(8,128)} fusion(bf16[512,512]{1,0:T(8,128)(2,1)S(1)} %bitcast.85, bf16[1,512,1024]{2,1,0:T(8,128)(2,1)S(1)} %copy-done.1), kind=kOutput, calls=%fused_computation.20 | convolution fusion | flops 536870912 | bytes 3670016 | tf_op jit(solution)/shard_map/dot_general | solution.py:70
  38.9 0.8 copy.87
  39.9 45.8 %all-gather.2.cloned.1.call-done = bf16[1024,2048]{1,0:T(8,128)(2,1)} async-done(((bf16[128,2048]{1,0:T(8,128)(2,1)}), bf16[1024,2048]{1,0:T(8,128)(2,1)}) %all-gather.2.cloned.1.call-update) | async-done | bytes 4194320 | tf_op jit(solution)/shard_map/all_gather | solution.py:61
  85.7 3.7 %fusion.14 = bf16[1,128,1024]{2,1,0:T(8,128)(2,1)S(1)} fusion(bf16[1024,2048]{1,0:T(8,128)(2,1)} %all-gather.2.cloned.1.call-done, bf16[1,128,2048]{2,1,0:T(8,128)(2,1)S(1)} %copy-done), kind=kOutput, calls=%fused_computation.19 | convolution fusion | flops 537001984 | bytes 4980736 | tf_op jit(solution)/shard_map/dot_general | solution.py:59
  89.8 2.2 %reduce = bf16[1024,128]{1,0:T(8,128)(2,1)S(1)} reduce(bf16[1024,1,128]{2,1,0:T(2,128)(2,1)S(1)} %bitcast.92, bf16[]{:T(256)} %broadcast.48), dimensions={1}, to_apply=%bitcast.59.reduce_sub_computation | reduce | bytes 524290
  92.0 0.8 reshape.71
  92.8 3.6 %all-to-all-start = ((bf16[4,2,16384]{2,1,0:T(2,128)(2,1)}), bf16[4,2,16384]{2,1,0:T(2,128)(2,1)S(1)}, u32[]{:S(2)}, u32[]{:S(2)}) async-start(bf16[4,2,16384]{2,1,0:T(2,128)(2,1)} %reshape.71), calls=%async_computation | async-start | bytes 524288 | tf_op jit(solution)/shard_map/all_to_all | solution.py:66
  96.4 3.4 %fusion.32 = (f32[4,512]{1,0:T(4,128)S(1)}, f32[4,512,512]{1,2,0:T(8,128)}) fusion(f32[4,512]{1,0:T(4,128)S(1)} %bitcast.112, pred[512,512]{0,1:T(8,128)(4,1)S(1)} %iota_compare_fusion, bf16[4,512,64]{1,2,0:T(8,128)(2,1)S(1)} %bitcast.97, bf16[4,512,64]{1,2,0:T(8,128)(2,1)S(1)} %bitcast.100), kind=kOutput, calls=%fused_computation.38 | convolution fusion | flops 140509696 | bytes 4997120 | tf_op jit(solution)/shard_map/while/body/eval_jaxpr/sub | solution.py:30
  99.8 2.3 %all-to-all-done = bf16[4,2,16384]{2,1,0:T(2,128)(2,1)S(1)} async-done(((bf16[4,2,16384]{2,1,0:T(2,128)(2,1)}), bf16[4,2,16384]{2,1,0:T(2,128)(2,1)S(1)}, u32[]{:S(2)}, u32[]{:S(2)}) %all-to-all-start) | async-done | bytes 262176 | tf_op jit(solution)/shard_map/all_to_all | solution.py:66
  102.9 3.5 %fusion.31 = (f32[4,512]{1,0:T(4,128)S(1)}, f32[4,512]{1,0:T(4,128)S(1)}, bf16[4,512,512]{1,2,0:T(8,128)(2,1)S(1)}) fusion(f32[4,512]{1,0:T(4,128)S(1)} %multiply_reduce_fusion, bf16[4,512,64]{1,2,0:T(8,128)(2,1)} %bitcast.111, bf16[512,4,64]{0,2,1:T(8,128)(2,1)S(1)} %reshape_squeeze.14, f32[4,512,512]{1,2,0:T(8,128)} %get-tuple-element.52, ...), kind=kOutput, calls=%fused_computation.37 | convolution fusion | flops 140505088 | bytes 6848512 | tf_op jit(solution)/shard_map/while/body/eval_jaxpr/hqe,hke->hqk/dot_general | solution.py:15
  106.4 0.8 fusion.9
  107.6 3.0 %reduce.2 = bf16[512,256]{1,0:T(8,128)(2,1)} reduce(bf16[512,1,256]{2,1,0:T(2,128)(2,1)S(1)} %bitcast.93, bf16[]{:T(256)} %broadcast.48), dimensions={1}, to_apply=%bitcast.63.reduce_sub_computation | reduce | bytes 524290
  110.6 1.7 %reshape.75 = bf16[4,2,16384]{2,1,0:T(2,128)(2,1)} reshape(bf16[512,256]{1,0:T(8,128)(2,1)} %reduce.2) | data formatting | bytes 524288
  112.3 3.4 %all-to-all-start.2 = ((bf16[4,2,16384]{2,1,0:T(2,128)(2,1)}), bf16[4,2,16384]{2,1,0:T(2,128)(2,1)S(1)}, u32[]{:S(2)}, u32[]{:S(2)}) async-start(bf16[4,2,16384]{2,1,0:T(2,128)(2,1)} %reshape.75), calls=%async_computation.2 | async-start | bytes 524288 | tf_op jit(solution)/shard_map/all_to_all | solution.py:104
  116.6 2.2 %reduce.1 = bf16[512,256]{1,0:T(8,128)(2,1)S(1)} reduce(bf16[512,1,256]{2,1,0:T(2,128)(2,1)S(1)} %bitcast.94, bf16[]{:T(256)} %broadcast.48), dimensions={1}, to_apply=%bitcast.61.reduce_sub_computation | reduce | bytes 524290
  118.8 0.8 reshape.73
  119.6 2.1 %all-to-all-done.2 = bf16[4,2,16384]{2,1,0:T(2,128)(2,1)S(1)} async-done(((bf16[4,2,16384]{2,1,0:T(2,128)(2,1)}), bf16[4,2,16384]{2,1,0:T(2,128)(2,1)S(1)}, u32[]{:S(2)}, u32[]{:S(2)}) %all-to-all-start.2) | async-done | bytes 262176 | tf_op jit(solution)/shard_map/all_to_all | solution.py:104
  121.7 3.4 %all-to-all-start.1 = ((bf16[4,2,16384]{2,1,0:T(2,128)(2,1)}), bf16[4,2,16384]{2,1,0:T(2,128)(2,1)S(1)}, u32[]{:S(2)}, u32[]{:S(2)}) async-start(bf16[4,2,16384]{2,1,0:T(2,128)(2,1)} %reshape.73), calls=%async_computation.1 | async-start | bytes 524288 | tf_op jit(solution)/shard_map/all_to_all | solution.py:103
  125.1 3.2 %fusion.11 = bf16[4,512,64]{1,2,0:T(8,128)(2,1)S(1)} fusion(f32[4,512]{1,0:T(4,128)S(1)} %get-tuple-element.38, bf16[512,4,64]{0,2,1:T(8,128)(2,1)S(1)} %copy-done.3, f32[4,512]{1,0:T(4,128)S(1)} %bitcast.113, pred[512,512]{0,1:T(8,128)(4,1)} %copy-done.7, bf16[4,512,64]{1,2,0:T(8,128)(2,1)S(1)} %bitcast.99, bf16[4,512,64]{1,2,0:T(8,128)(2,1)S(1)} %bitcast.102), kind=kOutput, calls=%fused_computation.18 | convolution fusion | flops 275909120 | bytes 1327104 | tf_op jit(solution)/shard_map/while/body/eval_jaxpr/hqk,hqe->hke/dot_general | solution.py:15
  128.8 2.2 %reduce.3 = bf16[512,256]{1,0:T(8,128)(2,1)S(1)} reduce(bf16[512,1,256]{2,1,0:T(2,128)(2,1)S(1)} %bitcast.91, bf16[]{:T(256)} %broadcast.48), dimensions={1}, to_apply=%bitcast.65.reduce_sub_computation | reduce | bytes 524290
  131.0 0.8 reshape.77
  131.7 3.4 %all-to-all-start.3 = ((bf16[4,2,16384]{2,1,0:T(2,128)(2,1)}), bf16[4,2,16384]{2,1,0:T(2,128)(2,1)S(1)}, u32[]{:S(2)}, u32[]{:S(2)}) async-start(bf16[4,2,16384]{2,1,0:T(2,128)(2,1)} %reshape.77), calls=%async_computation.3 | async-start | bytes 524288 | tf_op jit(solution)/shard_map/all_to_all | solution.py:105
  135.2 0.6 add_bitcast_fusion
  136.3 0.9 copy.102
  137.6 0.9 copy.101
  138.5 2.7 %all-to-all-done.3 = bf16[4,2,16384]{2,1,0:T(2,128)(2,1)S(1)} async-done(((bf16[4,2,16384]{2,1,0:T(2,128)(2,1)}), bf16[4,2,16384]{2,1,0:T(2,128)(2,1)S(1)}, u32[]{:S(2)}, u32[]{:S(2)}) %all-to-all-start.3) | async-done | bytes 262176 | tf_op jit(solution)/shard_map/all_to_all | solution.py:105
  141.6 0.9 copy.103
  142.5 14.2 %reduce-scatter.2.cloned.1.call-done = f32[128,512]{1,0:T(8,128)} async-done(((f32[1024,512]{1,0:T(8,128)}), f32[128,512]{1,0:T(8,128)}) %reduce-scatter.2.cloned.1.call-update) | async-done | bytes 262160 | tf_op jit(solution)/shard_map/reduce_scatter | solution.py:69
  (51 shorter events, 6.5 us)
Async XLA Ops:
  7.2 78.5 %all-gather.2.cloned.1.call-start = ((), (), s32[]{:S(2)}) async-start(), calls=%async_computation.6 | async-start | bytes 4718592 | tf_op jit(solution)/shard_map/all_gather | solution.py:61
  7.9 148.7 %reduce-scatter.2.cloned.1.call-start = ((), (), s32[]{:S(2)}) async-start(), calls=%async_computation.7 | async-start | bytes 2359296 | tf_op jit(solution)/shard_map/reduce_scatter | solution.py:69
  10.3 25.9 %copy-start.1 = (bf16[1,512,1024]{2,1,0:T(8,128)(2,1)S(1)}, bf16[1,512,1024]{2,1,0:T(8,128)(2,1)}, u32[]{:S(2)}) copy-start(bf16[1,512,1024]{2,1,0:T(8,128)(2,1)} %param.10) | copy-start | bytes 3145732
  35.9 2.6 %copy-start.4 = (bf16[1,512,256]{2,1,0:T(8,128)(2,1)S(1)}, bf16[1,512,256]{2,1,0:T(8,128)(2,1)}, u32[]{:S(2)}) copy-start(bf16[1,512,256]{2,1,0:T(8,128)(2,1)} %param.7) | copy-start | bytes 786436
  36.2 2.6 %copy-start.5 = (bf16[1,512,256]{2,1,0:T(8,128)(2,1)S(1)}, bf16[1,512,256]{2,1,0:T(8,128)(2,1)}, u32[]{:S(2)}) copy-start(bf16[1,512,256]{2,1,0:T(8,128)(2,1)} %param.8) | copy-start | bytes 786436
  36.2 2.7 %copy-start.6 = (bf16[1,512,256]{2,1,0:T(8,128)(2,1)S(1)}, bf16[1,512,256]{2,1,0:T(8,128)(2,1)}, u32[]{:S(2)}) copy-start(bf16[1,512,256]{2,1,0:T(8,128)(2,1)} %param.9) | copy-start | bytes 786436
  36.2 49.5 %copy-start = (bf16[1,128,2048]{2,1,0:T(8,128)(2,1)S(1)}, bf16[1,128,2048]{2,1,0:T(8,128)(2,1)}, u32[]{:S(2)}) copy-start(bf16[1,128,2048]{2,1,0:T(8,128)(2,1)} %param.12) | copy-start | bytes 1572868
  38.9 57.5 %copy-start.8 = (f32[1,4,512]{2,1,0:T(4,128)S(1)}, f32[1,4,512]{2,1,0:T(4,128)}, u32[]{:S(2)}) copy-start(f32[1,4,512]{2,1,0:T(4,128)} %param.11) | copy-start | bytes 24580
  39.9 60.0 %copy-start.7 = (pred[512,512]{0,1:T(8,128)(4,1)}, pred[512,512]{0,1:T(8,128)(4,1)S(1)}, u32[]{:S(2)}) copy-start(pred[512,512]{0,1:T(8,128)(4,1)S(1)} %iota_compare_fusion) | copy-start | bytes 786436
  92.8 9.4 %all-to-all-start = ((bf16[4,2,16384]{2,1,0:T(2,128)(2,1)}), bf16[4,2,16384]{2,1,0:T(2,128)(2,1)S(1)}, u32[]{:S(2)}, u32[]{:S(2)}) async-start(bf16[4,2,16384]{2,1,0:T(2,128)(2,1)} %reshape.71), calls=%async_computation | async-start | bytes 524288 | tf_op jit(solution)/shard_map/all_to_all | solution.py:66
  102.8 3.6 %copy-start.2 = (bf16[512,4,64]{0,2,1:T(8,128)(2,1)}, bf16[512,4,64]{0,2,1:T(8,128)(2,1)S(1)}, u32[]{:S(2)}) copy-start(bf16[512,4,64]{0,2,1:T(8,128)(2,1)S(1)} %reshape_squeeze.14) | copy-start | bytes 786436
  107.6 17.5 %copy-start.3 = (bf16[512,4,64]{0,2,1:T(8,128)(2,1)S(1)}, bf16[512,4,64]{0,2,1:T(8,128)(2,1)}, u32[]{:S(2)}) copy-start(bf16[512,4,64]{0,2,1:T(8,128)(2,1)} %copy-done.2) | copy-start | bytes 786436
  112.3 9.4 %all-to-all-start.2 = ((bf16[4,2,16384]{2,1,0:T(2,128)(2,1)}), bf16[4,2,16384]{2,1,0:T(2,128)(2,1)S(1)}, u32[]{:S(2)}, u32[]{:S(2)}) async-start(bf16[4,2,16384]{2,1,0:T(2,128)(2,1)} %reshape.75), calls=%async_computation.2 | async-start | bytes 524288 | tf_op jit(solution)/shard_map/all_to_all | solution.py:104
  121.7 10.1 %all-to-all-start.1 = ((bf16[4,2,16384]{2,1,0:T(2,128)(2,1)}), bf16[4,2,16384]{2,1,0:T(2,128)(2,1)S(1)}, u32[]{:S(2)}, u32[]{:S(2)}) async-start(bf16[4,2,16384]{2,1,0:T(2,128)(2,1)} %reshape.73), calls=%async_computation.1 | async-start | bytes 524288 | tf_op jit(solution)/shard_map/all_to_all | solution.py:103
  131.7 9.4 %all-to-all-start.3 = ((bf16[4,2,16384]{2,1,0:T(2,128)(2,1)}), bf16[4,2,16384]{2,1,0:T(2,128)(2,1)S(1)}, u32[]{:S(2)}, u32[]{:S(2)}) async-start(bf16[4,2,16384]{2,1,0:T(2,128)(2,1)} %reshape.77), calls=%async_computation.3 | async-start | bytes 524288 | tf_op jit(solution)/shard_map/all_to_all | solution.py:105
Sparse Core Ops, SparseCore 0:
  10.1 75.5 all-gather.1
  89.8 66.8 reduce-scatter.1
where the time goes:
time: 164 us; the launch traced here: 163 us
  waiting for transfers between devices  67.7 us (41%)
  other arithmetic  21.9 us (13%)
  matrix products  17.1 us (10%)
  local copies, waits for them, and re-layouts  15.5 us (9%)
  between operations  14.5 us (9%)
  starting transfers between devices  13.9 us (8%)
  blocking collectives  12.9 us (8%)
    all_gather x1, waiting for transfers between devices, shards(): lax.all_gather(w_out, 'dp', axis=0, tiled=True)  45.8 us
    unnamed x5, other arithmetic  21.1 us
    reduce_scatter x1, waiting for transfers between devices, shards(): lax.psum_scatter(lax.dot_general(whole_output, column_part[0], (((0,), (0...  14.2 us
    all_to_all x1, blocking collectives, shards(): lax.all_to_all(d_out, 'sp', split_axis=2, concat_axis=1, tiled=True)  12.9 us
    unnamed x41, local copies, waits for them, and re-layouts  12.5 us
    dot_general x4, matrix products, product(): return jnp.einsum(form, left, right, preferred_element_type=jnp.float32)  7.92 us
    dot_general x1, matrix products, shards(): lax.dot_general(local_rows, lax.all_gather(w_out, 'dp', axis=0, tiled=Tru...  3.7 us
    all_to_all x1, starting transfers between devices, shards(): lax.all_to_all(d_attn[None], 'sp', split_axis=2, concat_axis=1, tiled=True)  3.6 us
  transfers between devices with their start and end apart: 6, of which 5 were waited for; matrix products, arithmetic and copies ran while one was open for 33% of the time, Pallas kernels for 0%

commit v1 on v0

--- a/solution.py
+++ b/solution.py
@@ -2,6 +2,13 @@
 import jax.numpy as jnp
 from jax import lax
 from jax.sharding import PartitionSpec as P
+
+
+def swap_blocks(value, axis, split, join):
+    peers = lax.axis_size(axis)
+    pieces = jnp.stack(jnp.split(value, peers, axis=split), axis=0)
+    pieces = lax.all_to_all(pieces, axis, split_axis=0, concat_axis=0)
+    return jnp.concatenate(pieces, axis=join)
 
 
 def head_grads(query, keys, values, output, cotangent, cum):
@@ -64,7 +71,7 @@
     ).astype(jnp.bfloat16)
     head_cot, column_part = (
         lax.all_to_all(d_attn[None], "sp", split_axis=2, concat_axis=1, tiled=True),
-        lax.all_to_all(d_out, "sp", split_axis=2, concat_axis=1, tiled=True),
+        swap_blocks(d_out, "sp", 2, 1),
     )
     grad_weight = lax.psum_scatter(
         lax.dot_general(

time: 164 us -> 206 us (1.26)
  waiting for transfers between devices: 67.7 us -> 122 us
  other arithmetic: 21.9 us -> 10.5 us
    reduce_scatter x1, waiting for transfers between devices: 14.2 us -> 56.5 us  [shards(): lax.psum_scatter(lax.dot_general(whole_output, column_part[0], (((0,), (0...]
    all_gather x1, waiting for transfers between devices: 45.8 us -> 59.9 us  [shards(): lax.all_gather(w_out, 'dp', axis=0, tiled=True)]
    unnamed x5 -> x4, other arithmetic: 21.1 us -> 9.59 us
    all_to_all x1, waiting for transfers between devices: 2.34 us -> 0.01 us  [shards(): lax.all_to_all(d_attn[None], 'sp', split_axis=2, concat_axis=1, tiled=True)]
    unnamed x41 -> x38, local copies, waits for them, and re-layouts: 12.5 us -> 11.3 us
  transfers between devices with their start and end apart: 6 -> 6, of which waited for: 5 -> 4; matrix products, arithmetic and copies ran while one was open for 33% -> 15% of each run, Pallas kernels for 0% -> 0%
where the time goes in v1:
time: 206 us
  waiting for transfers between devices  122 us (59%)
  matrix products  17.1 us (8%)
  local copies, waits for them, and re-layouts  15.1 us (7%)
  between operations  14.4 us (7%)
  starting transfers between devices  13.9 us (7%)
  blocking collectives  13 us (6%)
  other arithmetic  10.5 us (5%)
    all_gather x1, waiting for transfers between devices, shards(): lax.all_gather(w_out, 'dp', axis=0, tiled=True)  59.9 us
    reduce_scatter x1, waiting for transfers between devices, shards(): lax.psum_scatter(lax.dot_general(whole_output, column_part[0], (((0,), (0...  56.5 us
    all_to_all x1, blocking collectives, swap_blocks(): pieces = lax.all_to_all(pieces, axis, split_axis=0, concat_axis=0)  13 us
    unnamed x38, local copies, waits for them, and re-layouts  11.3 us
    unnamed x4, other arithmetic  9.59 us
    dot_general x4, matrix products, product(): return jnp.einsum(form, left, right, preferred_element_type=jnp.float32)  7.89 us
  transfers between devices with their start and end apart: 6, of which 4 were waited for; matrix products, arithmetic and copies ran while one was open for 15% of the time, Pallas kernels for 0%

profile of v1, /device:TPU:0, one launch (start us, length us, event | category | flops | bytes accessed | tf_op | source)
XLA Modules:
  0.0 205.6 jit_solution(14533844079328939834)
XLA Ops:
  7.2 0.7 all-gather.2.cloned.1.call-update
  8.0 1.1 slice_bitcast_fusion.3
  9.2 13.0 %all_to_all.74 = bf16[4,1,128,512]{3,2,1,0:T(8,128)(2,1)S(1)} all-to-all(bf16[4,1,128,512]{3,2,1,0:T(8,128)(2,1)S(1)} %pad_maximum_fusion), channel_id=1, replica_groups=mesh['sp'=4,'dp'=8] {'sp'}, dimensions={0} | all-to-all | bytes 1048576 | tf_op jit(solution)/shard_map/all_to_all | solution.py:10
  22.2 2.1 convolution_bitcast_fusion
  24.9 0.8 copy.73
  25.8 59.9 %all-gather.2.cloned.1.call-done = bf16[1024,2048]{1,0:T(8,128)(2,1)} async-done(((bf16[128,2048]{1,0:T(8,128)(2,1)}), bf16[1024,2048]{1,0:T(8,128)(2,1)}) %all-gather.2.cloned.1.call-update) | async-done | bytes 4194320 | tf_op jit(solution)/shard_map/all_gather | solution.py:68
  85.7 3.7 %fusion.14 = bf16[1,128,1024]{2,1,0:T(8,128)(2,1)S(1)} fusion(bf16[1024,2048]{1,0:T(8,128)(2,1)} %all-gather.2.cloned.1.call-done, bf16[1,128,2048]{2,1,0:T(8,128)(2,1)S(1)} %copy-done), kind=kOutput, calls=%fused_computation.20 | convolution fusion | flops 537001984 | bytes 4980736 | tf_op jit(solution)/shard_map/dot_general | solution.py:66
  89.8 0.5 broadcast.48
  90.3 2.2 %reduce = bf16[1024,128]{1,0:T(8,128)(2,1)S(1)} reduce(bf16[1024,1,128]{2,1,0:T(2,128)(2,1)S(1)} %bitcast.93, bf16[]{:T(256)} %broadcast.48), dimensions={1}, to_apply=%bitcast.66.reduce_sub_computation | reduce | bytes 524290
  92.5 0.8 reshape.70
  93.3 3.4 %all-to-all-start = ((bf16[4,2,16384]{2,1,0:T(2,128)(2,1)}), bf16[4,2,16384]{2,1,0:T(2,128)(2,1)S(1)}, u32[]{:S(2)}, u32[]{:S(2)}) async-start(bf16[4,2,16384]{2,1,0:T(2,128)(2,1)} %reshape.70), calls=%async_computation | async-start | bytes 524288 | tf_op jit(solution)/shard_map/all_to_all | solution.py:73
  96.7 3.4 %fusion.31 = (f32[4,512]{1,0:T(4,128)S(1)}, f32[4,512,512]{1,2,0:T(8,128)}) fusion(f32[4,512]{1,0:T(4,128)S(1)} %bitcast.114, pred[512,512]{0,1:T(8,128)(4,1)S(1)} %iota_compare_fusion, bf16[4,512,64]{1,2,0:T(8,128)(2,1)S(1)} %bitcast.99, bf16[4,512,64]{1,2,0:T(8,128)(2,1)S(1)} %bitcast.102), kind=kOutput, calls=%fused_computation.43 | convolution fusion | flops 140509696 | bytes 4997120 | tf_op jit(solution)/shard_map/while/body/eval_jaxpr/sub | solution.py:37
  100.1 56.5 %reduce-scatter.2.cloned.1.call-done = f32[128,512]{0,1:T(8,128)} async-done(((f32[1024,512]{0,1:T(8,128)}), f32[128,512]{0,1:T(8,128)}) %reduce-scatter.2.cloned.1.call-update) | async-done | bytes 262160 | tf_op jit(solution)/shard_map/reduce_scatter | solution.py:76
  156.6 1.8 copy.88
  159.2 3.5 %fusion.30 = (f32[4,512]{1,0:T(4,128)S(1)}, f32[4,512]{1,0:T(4,128)S(1)}, bf16[4,512,512]{1,2,0:T(8,128)(2,1)S(1)}) fusion(f32[4,512]{1,0:T(4,128)S(1)} %multiply_reduce_fusion, bf16[4,512,64]{1,2,0:T(8,128)(2,1)} %bitcast.113, bf16[512,4,64]{0,2,1:T(8,128)(2,1)S(1)} %reshape_squeeze.14, f32[4,512,512]{1,2,0:T(8,128)} %get-tuple-element.76, ...), kind=kOutput, calls=%fused_computation.42 | convolution fusion | flops 140505088 | bytes 6848512 | tf_op jit(solution)/shard_map/while/body/eval_jaxpr/hqe,hke->hqk/dot_general | solution.py:22
  162.6 0.8 fusion.9
  163.8 3.0 %reduce.2 = bf16[512,256]{1,0:T(8,128)(2,1)} reduce(bf16[512,1,256]{2,1,0:T(2,128)(2,1)S(1)} %bitcast.95, bf16[]{:T(256)} %broadcast.48), dimensions={1}, to_apply=%bitcast.70.reduce_sub_computation | reduce | bytes 524290
  166.8 1.7 reshape.74
  168.5 3.6 %all-to-all-start.2 = ((bf16[4,2,16384]{2,1,0:T(2,128)(2,1)}), bf16[4,2,16384]{2,1,0:T(2,128)(2,1)S(1)}, u32[]{:S(2)}, u32[]{:S(2)}) async-start(bf16[4,2,16384]{2,1,0:T(2,128)(2,1)} %reshape.74), calls=%async_computation.2 | async-start | bytes 524288 | tf_op jit(solution)/shard_map/all_to_all | solution.py:111
  173.0 2.2 %reduce.1 = bf16[512,256]{1,0:T(8,128)(2,1)S(1)} reduce(bf16[512,1,256]{2,1,0:T(2,128)(2,1)S(1)} %bitcast.96, bf16[]{:T(256)} %broadcast.48), dimensions={1}, to_apply=%bitcast.68.reduce_sub_computation | reduce | bytes 524290
  175.2 0.8 reshape.72
  176.0 1.9 all-to-all-done.2
  177.9 3.4 %all-to-all-start.1 = ((bf16[4,2,16384]{2,1,0:T(2,128)(2,1)}), bf16[4,2,16384]{2,1,0:T(2,128)(2,1)S(1)}, u32[]{:S(2)}, u32[]{:S(2)}) async-start(bf16[4,2,16384]{2,1,0:T(2,128)(2,1)} %reshape.72), calls=%async_computation.1 | async-start | bytes 524288 | tf_op jit(solution)/shard_map/all_to_all | solution.py:110
  181.3 3.2 %fusion.11 = bf16[4,512,64]{1,2,0:T(8,128)(2,1)S(1)} fusion(f32[4,512]{1,0:T(4,128)S(1)} %get-tuple-element.75, bf16[512,4,64]{0,2,1:T(8,128)(2,1)S(1)} %copy-done.3, f32[4,512]{1,0:T(4,128)S(1)} %bitcast.115, pred[512,512]{0,1:T(8,128)(4,1)} %copy-done.7, bf16[4,512,64]{1,2,0:T(8,128)(2,1)S(1)} %bitcast.101, bf16[4,512,64]{1,2,0:T(8,128)(2,1)S(1)} %bitcast.104), kind=kOutput, calls=%fused_computation.19 | convolution fusion | flops 275909120 | bytes 1327104 | tf_op jit(solution)/shard_map/while/body/eval_jaxpr/hqk,hqe->hke/dot_general | solution.py:22
  185.0 2.2 %reduce.3 = bf16[512,256]{1,0:T(8,128)(2,1)S(1)} reduce(bf16[512,1,256]{2,1,0:T(2,128)(2,1)S(1)} %bitcast.94, bf16[]{:T(256)} %broadcast.48), dimensions={1}, to_apply=%bitcast.72.reduce_sub_computation | reduce | bytes 524290
  187.2 0.8 reshape.76
  188.0 3.4 %all-to-all-start.3 = ((bf16[4,2,16384]{2,1,0:T(2,128)(2,1)}), bf16[4,2,16384]{2,1,0:T(2,128)(2,1)S(1)}, u32[]{:S(2)}, u32[]{:S(2)}) async-start(bf16[4,2,16384]{2,1,0:T(2,128)(2,1)} %reshape.76), calls=%async_computation.3 | async-start | bytes 524288 | tf_op jit(solution)/shard_map/all_to_all | solution.py:112
  191.4 0.6 add_bitcast_fusion
  192.5 0.9 copy.86
  193.8 0.9 copy.85
  194.7 2.7 %all-to-all-done.3 = bf16[4,2,16384]{2,1,0:T(2,128)(2,1)S(1)} async-done(((bf16[4,2,16384]{2,1,0:T(2,128)(2,1)}), bf16[4,2,16384]{2,1,0:T(2,128)(2,1)S(1)}, u32[]{:S(2)}, u32[]{:S(2)}) %all-to-all-start.3) | async-done | bytes 262176 | tf_op jit(solution)/shard_map/all_to_all | solution.py:112
  197.9 0.9 copy.87
  (48 shorter events, 5.1 us)
Async XLA Ops:
  7.2 15.0 %copy-start.1 = (bf16[1,512,1024]{2,1,0:T(8,128)(2,1)S(1)}, bf16[1,512,1024]{2,1,0:T(8,128)(2,1)}, u32[]{:S(2)}) copy-start(bf16[1,512,1024]{2,1,0:T(8,128)(2,1)} %param.10) | copy-start | bytes 3145732
  7.2 78.5 %all-gather.2.cloned.1.call-start = ((), (), s32[]{:S(2)}) async-start(), calls=%async_computation.6 | async-start | bytes 4718592 | tf_op jit(solution)/shard_map/all_gather | solution.py:68
  7.9 148.7 %reduce-scatter.2.cloned.1.call-start = ((), (), s32[]{:S(2)}) async-start(), calls=%async_computation.7 | async-start | bytes 2359296 | tf_op jit(solution)/shard_map/reduce_scatter | solution.py:76
  9.2 15.3 %copy-start.4 = (bf16[1,512,256]{2,1,0:T(8,128)(2,1)S(1)}, bf16[1,512,256]{2,1,0:T(8,128)(2,1)}, u32[]{:S(2)}) copy-start(bf16[1,512,256]{2,1,0:T(8,128)(2,1)} %param.7) | copy-start | bytes 786436
  22.2 2.5 %copy-start.5 = (bf16[1,512,256]{2,1,0:T(8,128)(2,1)S(1)}, bf16[1,512,256]{2,1,0:T(8,128)(2,1)}, u32[]{:S(2)}) copy-start(bf16[1,512,256]{2,1,0:T(8,128)(2,1)} %param.8) | copy-start | bytes 786436
  22.2 2.7 %copy-start.6 = (bf16[1,512,256]{2,1,0:T(8,128)(2,1)S(1)}, bf16[1,512,256]{2,1,0:T(8,128)(2,1)}, u32[]{:S(2)}) copy-start(bf16[1,512,256]{2,1,0:T(8,128)(2,1)} %param.9) | copy-start | bytes 786436
  22.2 63.5 %copy-start = (bf16[1,128,2048]{2,1,0:T(8,128)(2,1)S(1)}, bf16[1,128,2048]{2,1,0:T(8,128)(2,1)}, u32[]{:S(2)}) copy-start(bf16[1,128,2048]{2,1,0:T(8,128)(2,1)} %param.12) | copy-start | bytes 1572868
  24.8 71.9 %copy-start.8 = (f32[1,4,512]{2,1,0:T(4,128)S(1)}, f32[1,4,512]{2,1,0:T(4,128)}, u32[]{:S(2)}) copy-start(f32[1,4,512]{2,1,0:T(4,128)} %param.11) | copy-start | bytes 24580
  25.8 74.4 %copy-start.7 = (pred[512,512]{0,1:T(8,128)(4,1)}, pred[512,512]{0,1:T(8,128)(4,1)S(1)}, u32[]{:S(2)}) copy-start(pred[512,512]{0,1:T(8,128)(4,1)S(1)} %iota_compare_fusion) | copy-start | bytes 786436
  93.3 65.2 %all-to-all-start = ((bf16[4,2,16384]{2,1,0:T(2,128)(2,1)}), bf16[4,2,16384]{2,1,0:T(2,128)(2,1)S(1)}, u32[]{:S(2)}, u32[]{:S(2)}) async-start(bf16[4,2,16384]{2,1,0:T(2,128)(2,1)} %reshape.70), calls=%async_computation | async-start | bytes 524288 | tf_op jit(solution)/shard_map/all_to_all | solution.py:73
  159.1 3.6 %copy-start.2 = (bf16[512,4,64]{0,2,1:T(8,128)(2,1)}, bf16[512,4,64]{0,2,1:T(8,128)(2,1)S(1)}, u32[]{:S(2)}) copy-start(bf16[512,4,64]{0,2,1:T(8,128)(2,1)S(1)} %reshape_squeeze.14) | copy-start | bytes 786436
  163.8 17.5 %copy-start.3 = (bf16[512,4,64]{0,2,1:T(8,128)(2,1)S(1)}, bf16[512,4,64]{0,2,1:T(8,128)(2,1)}, u32[]{:S(2)}) copy-start(bf16[512,4,64]{0,2,1:T(8,128)(2,1)} %copy-done.2) | copy-start | bytes 786436
  168.5 9.4 %all-to-all-start.2 = ((bf16[4,2,16384]{2,1,0:T(2,128)(2,1)}), bf16[4,2,16384]{2,1,0:T(2,128)(2,1)S(1)}, u32[]{:S(2)}, u32[]{:S(2)}) async-start(bf16[4,2,16384]{2,1,0:T(2,128)(2,1)} %reshape.74), calls=%async_computation.2 | async-start | bytes 524288 | tf_op jit(solution)/shard_map/all_to_all | solution.py:111
  177.9 10.1 %all-to-all-start.1 = ((bf16[4,2,16384]{2,1,0:T(2,128)(2,1)}), bf16[4,2,16384]{2,1,0:T(2,128)(2,1)S(1)}, u32[]{:S(2)}, u32[]{:S(2)}) async-start(bf16[4,2,16384]{2,1,0:T(2,128)(2,1)} %reshape.72), calls=%async_computation.1 | async-start | bytes 524288 | tf_op jit(solution)/shard_map/all_to_all | solution.py:110
  188.0 9.4 %all-to-all-start.3 = ((bf16[4,2,16384]{2,1,0:T(2,128)(2,1)}), bf16[4,2,16384]{2,1,0:T(2,128)(2,1)S(1)}, u32[]{:S(2)}, u32[]{:S(2)}) async-start(bf16[4,2,16384]{2,1,0:T(2,128)(2,1)} %reshape.76), calls=%async_computation.3 | async-start | bytes 524288 | tf_op jit(solution)/shard_map/all_to_all | solution.py:112
Sparse Core Ops, SparseCore 0:
  10.1 75.5 all-gather.1
  89.2 67.3 reduce-scatter.1
